TPU v7x, 256 devices: a whole 4x4x8 slice. The times are simulated.
256 devices in a mesh: ep: 64 (over z, y, core), tp: 4 (over x).
Axes of the slice: x: 4, y: 4, z: 8, core: 2. Of those that a mesh axis runs over, the one named last changes fastest.
Arguments:
- c_gate: bfloat16 [16384, 1024], P('ep', 'tp'), may hold values from -6 to 6
- b_gate: bfloat16 [16384, 1024], P('ep', 'tp'), may hold values from -6 to 6
- values: bfloat16 [16384, 1024], P('ep', 'tp'), may hold values from -6 to 6
- conv_taps: float32 [3, 1024], P(None, 'tp'), may hold values from -3.5 to 3.5
- w_mix_out: bfloat16 [1024, 2048], P('tp'), may hold values from -0.1875 to 0.1875
- moe_in: bfloat16 [32768, 2048], P(('ep', 'tp')), may hold values from -6 to 6
- norm_gain: float32 [2048], replicated, may hold values from 0.1 to 1.9
- route_ids: int32 [32768, 2], P(('ep', 'tp')), may hold values from 0 to 63, all different within a row; in each aligned block of 128 rows (0 to 127, 128 to 255, ...) at most 5 rows name the same one
- route_weights: float32 [32768, 2], P(('ep', 'tp')), may hold values from 0.1 to 1
- w_gate: bfloat16 [64, 2048, 3584], P('ep', None, 'tp'), may hold values from -0.125 to 0.125
- w_up: bfloat16 [64, 2048, 3584], P('ep', None, 'tp'), may hold values from -0.125 to 0.125
- w_down: bfloat16 [64, 3584, 2048], P('ep', 'tp'), may hold values from -0.09375 to 0.09375
Outputs:
- mixer_out: bfloat16 [16384, 2048], P(('ep', 'tp'))
- moe_out: bfloat16 [32768, 2048], P(('ep', 'tp'))
Inputs may be any that keep to these rules, and one draw needn't show every extreme that they name: `route_ids`: each row names 2 different experts; in each aligned block of 128 rows (the rows of one device) no expert is named by more than 5 rows, and in every draw some expert is named by exactly 5 rows in some block.
All inputs are finite; a program needn't handle non-finite values.
Results may differ from a plain program's by a relative error of at most 0.012.
Values may be sent and summed in bfloat16 or wider, within the bound.
No kernel may reach another device: no remote copies, remote signals or barrier semaphores. Data moves between devices by JAX's collectives and lax.ppermute only.
A program may use at most 128 MiB of HBM per device.

v0:
```python
import jax
import jax.numpy as jnp
from jax import lax
from jax.sharding import PartitionSpec as P

EPS = 1e-06


def passed_along(block, axis, distance):
    devices = range(lax.axis_size(axis))
    route = [(i - distance, i) for i in devices if i - distance in devices]
    return lax.ppermute(block, axis, route)


def split_up(shard, dim, length):
    before, after = (shard.shape[:dim], shard.shape[dim + 1 :])
    return jnp.moveaxis(shard.reshape(*before, length, -1, *after), dim, 0)


def sent_and_summed(shard, axis, dim):
    blocks = split_up(shard, dim, lax.axis_size(axis))
    arrived = lax.all_to_all(blocks, axis, split_axis=0, concat_axis=0, tiled=True)
    return arrived.astype(jnp.float32).sum(axis=0)


def rank_copies(route_block, experts):
    flat_ids = route_block.reshape(-1)
    onehot = (flat_ids[:, None] == jnp.arange(experts, dtype=jnp.int32)[None, :]).astype(jnp.int32)
    before = jnp.cumsum(onehot, axis=0) - onehot
    return (flat_ids, jnp.sum(before * onehot, axis=1))


def pack_rows(rows, slot_of, top, slot_count):
    copies = slot_of.shape[0]
    table = (
        jnp.full((slot_count,), copies, jnp.int32)
        .at[slot_of]
        .set(jnp.arange(copies, dtype=jnp.int32))
    )
    padded = jnp.concatenate([rows, jnp.zeros((1, rows.shape[1]), rows.dtype)], 0)
    return padded[table // top]


def on_device(
    c_gate,
    b_gate,
    values,
    conv_taps,
    w_mix_out,
    moe_in,
    norm_gain,
    route_ids,
    route_weights,
    w_gate,
    w_up,
    w_down,
):
    tokens = c_gate.shape[0]
    reach = conv_taps.shape[0] - 1
    product = c_gate.astype(jnp.float32) * values.astype(jnp.float32)
    previous = passed_along(product[tokens - reach :], "ep", 1)
    extended = jnp.concatenate([previous, product], 0)
    convolved = jnp.zeros_like(product)
    for offset in range(reach + 1):
        convolved = convolved + conv_taps[offset][None, :] * extended[offset : offset + tokens]
    mixed = (b_gate.astype(jnp.float32) * convolved).astype(jnp.bfloat16)
    piece = mixed
    mixer_out = sent_and_summed(
        jnp.dot(piece, w_mix_out, preferred_element_type=jnp.float32).astype(jnp.bfloat16), "tp", 0
    ).astype(jnp.bfloat16)
    rows_b = moe_in.shape[0]
    width = moe_in.shape[1]
    top = route_ids.shape[1]
    n_ep = lax.axis_size("ep")
    experts = w_gate.shape[0] * n_ep
    capacity = 5 * rows_b * top // (4 * experts)
    stream = moe_in.astype(jnp.float32)
    scale = lax.rsqrt(jnp.mean(stream * stream, axis=1, keepdims=True) + EPS)
    normed = (stream * scale * norm_gain[None, :]).astype(jnp.bfloat16)
    own_ids, own_ranks = rank_copies(route_ids, experts)
    own_slot = own_ids * capacity + own_ranks
    outgoing = pack_rows(normed, own_slot, top, experts * capacity).reshape(
        experts, capacity, width
    )
    arrived = lax.all_to_all(outgoing, "ep", split_axis=0, concat_axis=1, tiled=True).reshape(
        -1, width
    )
    piece = lax.all_gather(arrived, "tp", axis=0, tiled=True)
    gate_val = jnp.dot(piece, w_gate[0], preferred_element_type=jnp.float32)
    up_val = jnp.dot(piece, w_up[0], preferred_element_type=jnp.float32)
    hidden = (jax.nn.silu(gate_val) * up_val).astype(jnp.bfloat16)
    piece = hidden
    expert_out = sent_and_summed(
        jnp.dot(piece, w_down[0], preferred_element_type=jnp.float32).astype(jnp.bfloat16), "tp", 0
    ).astype(jnp.bfloat16)
    returned = lax.all_to_all(
        expert_out.reshape(n_ep, capacity, width), "ep", split_axis=0, concat_axis=0, tiled=True
    )
    picked = returned.reshape(-1, width)[own_slot].astype(jnp.float32).reshape(rows_b, top, width)
    moe_out = jnp.sum(picked * route_weights[:, :, None], axis=1).astype(jnp.bfloat16)
    return (mixer_out, moe_out)


def solution(mesh):
    return jax.shard_map(
        on_device,
        mesh=mesh,
        in_specs=(
            P("ep", "tp"),
            P("ep", "tp"),
            P("ep", "tp"),
            P(None, "tp"),
            P("tp", None),
            P(("ep", "tp"), None),
            P(),
            P(("ep", "tp"), None),
            P(("ep", "tp"), None),
            P("ep", None, "tp"),
            P("ep", None, "tp"),
            P("ep", "tp", None),
        ),
        out_specs=(P(("ep", "tp"), None), P(("ep", "tp"), None)),
        check_vma=False,
    )
```

profile of v0, /device:TPU:8, one launch (start us, length us, event | category | flops | bytes accessed | tf_op | source)
XLA Modules:
  0.0 333.2 jit_solution(17508996634302096302)
XLA Ops:
  10.3 1.4 scatter_custom_fusion
  13.0 1.2 fusion.6
  14.3 3.0 gather_fusion
  17.3 2.4 reshape.88
  19.7 63.2 %all_to_all.24 = bf16[64,5,2048]{2,1,0:T(8,128)(2,1)} all-to-all(bf16[64,5,2048]{2,1,0:T(8,128)(2,1)S(1)} %reshape.88), channel_id=1, replica_groups=mesh['ep'=64,'tp'=4] {'ep'}, dimensions={0} | all-to-all | bytes 2621440 | tf_op jit(solution)/shard_map/all_to_all | solution.py:85
  82.9 3.7 %reshape.89 = bf16[320,2048]{1,0:T(8,128)(2,1)} reshape(bf16[64,5,2048]{2,1,0:T(8,128)(2,1)} %all_to_all.24) | data formatting | bytes 2621440 | tf_op jit(solution)/shard_map/reshape | solution.py:85
  86.6 55.8 %all-gather.2.cloned.1.call-done = bf16[1280,2048]{1,0:T(8,128)(2,1)} async-done(((bf16[320,2048]{1,0:T(8,128)(2,1)}), bf16[1280,2048]{1,0:T(8,128)(2,1)}) %all-gather.2.cloned.1.call-update) | async-done | bytes 5242896 | tf_op jit(solution)/shard_map/all_gather | solution.py:88
  142.4 10.0 %fusion.2 = f32[1280,896]{1,0:T(8,128)} fusion(bf16[1280,2048]{1,0:T(8,128)(2,1)} %all-gather.2.cloned.1.call-done, bf16[1,2048,896]{2,1,0:T(8,128)(2,1)} %param.21), kind=kOutput, calls=%fused_computation.7 | convolution fusion | flops 4697620480 | bytes 13500416 | tf_op jit(solution)/shard_map/dot_general | solution.py:89
  152.4 17.5 %convolution_convert_fusion = bf16[1280,2048]{1,0:T(8,128)(2,1)} fusion(bf16[1,896,2048]{2,1,0:T(8,128)(2,1)} %param.23, f32[1280,896]{1,0:T(8,128)} %fusion.2, bf16[1280,2048]{1,0:T(8,128)(2,1)} %all-gather.2.cloned.1.call-done, bf16[1,2048,896]{2,1,0:T(8,128)(2,1)} %param.22), kind=kOutput, calls=%fused_computation.3 | convolution fusion | flops 9404743680 | bytes 22413312 | tf_op jit(solution)/shard_map/dot_general | solution.py:94
  169.9 5.2 %all-to-all-start.2 = ((bf16[4,320,2048]{2,1,0:T(8,128)(2,1)}), bf16[4,320,2048]{2,1,0:T(8,128)(2,1)}, u32[]{:S(2)}, u32[]{:S(2)}) async-start(bf16[4,320,2048]{2,1,0:T(8,128)(2,1)} %bitcast.47), calls=%async_computation.2 | async-start | bytes 10485760 | tf_op jit(solution)/shard_map/all_to_all | solution.py:22
  175.2 1.9 collective-permute-start
  177.2 3.0 collective-permute-done
  180.1 1.5 convolution_convert_fusion.1
  181.6 53.8 %all-to-all-done.2 = bf16[4,320,2048]{2,1,0:T(8,128)(2,1)} async-done(((bf16[4,320,2048]{2,1,0:T(8,128)(2,1)}), bf16[4,320,2048]{2,1,0:T(8,128)(2,1)}, u32[]{:S(2)}, u32[]{:S(2)}) %all-to-all-start.2) | async-done | bytes 5242912 | tf_op jit(solution)/shard_map/all_to_all | solution.py:22
  235.4 3.7 %all-to-all-start = ((bf16[4,64,2048]{2,1,0:T(8,128)(2,1)}), bf16[4,64,2048]{2,1,0:T(8,128)(2,1)S(1)}, u32[]{:S(2)}, u32[]{:S(2)}) async-start(bf16[4,64,2048]{2,1,0:T(8,128)(2,1)} %bitcast.3), calls=%async_computation | async-start | bytes 2097152 | tf_op jit(solution)/shard_map/all_to_all | solution.py:22
  239.1 3.6 %reduce_sum.57 = bf16[320,2048]{1,0:T(8,128)(2,1)S(1)} reduce(bf16[4,320,2048]{2,1,0:T(8,128)(2,1)} %all-to-all-done.2, bf16[]{:T(256)} %constant.18.clone.1), dimensions={0}, to_apply=%region_6.7 | reduce | flops 1966080 | bytes 6553602 | tf_op jit(solution)/shard_map/reduce_sum | solution.py:23
  242.7 1.6 reshape.91
  244.3 8.9 %all-to-all-done = bf16[4,64,2048]{2,1,0:T(8,128)(2,1)S(1)} async-done(((bf16[4,64,2048]{2,1,0:T(8,128)(2,1)}), bf16[4,64,2048]{2,1,0:T(8,128)(2,1)S(1)}, u32[]{:S(2)}, u32[]{:S(2)}) %all-to-all-start) | async-done | bytes 1048608 | tf_op jit(solution)/shard_map/all_to_all | solution.py:22
  253.2 10.7 %all-to-all-start.3 = ((bf16[64,5,2048]{2,1,0:T(8,128)(2,1)}), bf16[64,5,2048]{2,1,0:T(8,128)(2,1)}, u32[]{:S(2)}, u32[]{:S(2)}) async-start(bf16[64,5,2048]{2,1,0:T(8,128)(2,1)} %reshape.91), calls=%async_computation.3 | async-start | bytes 4194304 | tf_op jit(solution)/shard_map/all_to_all | solution.py:96
  265.0 50.1 %all-to-all-done.3 = bf16[64,5,2048]{2,1,0:T(8,128)(2,1)} async-done(((bf16[64,5,2048]{2,1,0:T(8,128)(2,1)}), bf16[64,5,2048]{2,1,0:T(8,128)(2,1)}, u32[]{:S(2)}, u32[]{:S(2)}) %all-to-all-start.3) | async-done | bytes 1310752 | tf_op jit(solution)/shard_map/all_to_all | solution.py:96
  315.1 2.6 reshape.92
  317.7 2.3 gather_fusion.1
  320.0 2.4 reshape.93
  322.4 3.9 %multiply_reduce_fusion = bf16[128,2048]{1,0:T(8,128)(2,1)} fusion(f32[128,2,2048]{2,1,0:T(2,128)S(1)} %reshape.93, f32[128,2]{1,0:T(8,128)S(1)} %copy.19), kind=kLoop, calls=%fused_computation.10 | loop fusion | flops 786432 | bytes 2622464 | tf_op jit(solution)/shard_map/reduce_sum | solution.py:100
  (39 shorter events, 5.5 us)
Async XLA Ops:
  7.2 173.0 %copy-start = (bf16[256,2048]{1,0:T(8,128)(2,1)S(1)}, bf16[256,2048]{1,0:T(8,128)(2,1)}, u32[]{:S(2)}) copy-start(bf16[256,2048]{1,0:T(8,128)(2,1)} %param.16) | copy-start | bytes 3145732
  7.2 135.2 %all-gather.2.cloned.1.call-start = ((), (), s32[]{:S(2)}) async-start(), calls=%async_computation.4 | async-start | bytes 6553600 | tf_op jit(solution)/shard_map/all_gather | solution.py:88
  169.9 5.3 %copy-start.2 = (bf16[256,256]{1,0:T(8,128)(2,1)S(1)}, bf16[256,256]{1,0:T(8,128)(2,1)}, u32[]{:S(2)}) copy-start(bf16[256,256]{1,0:T(8,128)(2,1)} %param.14) | copy-start | bytes 393220
  169.9 5.3 %copy-start.3 = (bf16[256,256]{1,0:T(8,128)(2,1)S(1)}, bf16[256,256]{1,0:T(8,128)(2,1)}, u32[]{:S(2)}) copy-start(bf16[256,256]{1,0:T(8,128)(2,1)} %param.12) | copy-start | bytes 393220
  169.9 7.2 %copy-start.4 = (f32[3,256]{1,0:T(4,128)S(1)}, f32[3,256]{1,0:T(4,128)}, u32[]{:S(2)}) copy-start(f32[3,256]{1,0:T(4,128)} %param.15) | copy-start | bytes 9220
  169.9 10.2 %copy-start.1 = (bf16[256,256]{1,0:T(8,128)(2,1)S(1)}, bf16[256,256]{1,0:T(8,128)(2,1)}, u32[]{:S(2)}) copy-start(bf16[256,256]{1,0:T(8,128)(2,1)} %param.13) | copy-start | bytes 393220
  169.9 65.4 %all-to-all-start.2 = ((bf16[4,320,2048]{2,1,0:T(8,128)(2,1)}), bf16[4,320,2048]{2,1,0:T(8,128)(2,1)}, u32[]{:S(2)}, u32[]{:S(2)}) async-start(bf16[4,320,2048]{2,1,0:T(8,128)(2,1)} %bitcast.47), calls=%async_computation.2 | async-start | bytes 10485760 | tf_op jit(solution)/shard_map/all_to_all | solution.py:22
  175.2 4.9 %collective-permute-start = (f32[2,256]{1,0:T(2,128)S(1)}, f32[2,256]{1,0:T(2,128)S(1)}, u32[]{:S(2)}, u32[]{:S(2)}) collective-permute-start(f32[2,256]{1,0:T(2,128)S(1)} %slice.36), channel_id=1, source_target_pairs={{0,4},{4,8},{8,12},{12,16},{16,20},{20,24},{24,28},{28,32},{32,36}... | collective-permute-start | bytes 6152 | tf_op jit(solution)/shard_map/ppermute | solution.py:12
  235.4 17.8 %all-to-all-start = ((bf16[4,64,2048]{2,1,0:T(8,128)(2,1)}), bf16[4,64,2048]{2,1,0:T(8,128)(2,1)S(1)}, u32[]{:S(2)}, u32[]{:S(2)}) async-start(bf16[4,64,2048]{2,1,0:T(8,128)(2,1)} %bitcast.3), calls=%async_computation | async-start | bytes 2097152 | tf_op jit(solution)/shard_map/all_to_all | solution.py:22
  242.7 21.3 %copy-start.5 = (f32[128,2]{0,1:T(2,128)S(1)}, f32[128,2]{0,1:T(2,128)}, u32[]{:S(2)}) copy-start(f32[128,2]{0,1:T(2,128)} %param.20) | copy-start | bytes 3076
  253.2 61.9 %all-to-all-start.3 = ((bf16[64,5,2048]{2,1,0:T(8,128)(2,1)}), bf16[64,5,2048]{2,1,0:T(8,128)(2,1)}, u32[]{:S(2)}, u32[]{:S(2)}) async-start(bf16[64,5,2048]{2,1,0:T(8,128)(2,1)} %reshape.91), calls=%async_computation.3 | async-start | bytes 4194304 | tf_op jit(solution)/shard_map/all_to_all | solution.py:96
Sparse Core Ops, SparseCore 0:
  86.7 55.6 all-gather.1
where the time goes:
time: 334 us; the launch traced here: 333 us
  waiting for transfers between devices  172 us (51%)
  blocking collectives  63.2 us (19%)
  matrix products  29 us (9%)
  starting transfers between devices  21.6 us (6%)
  local copies, waits for them, and re-layouts  21.1 us (6%)
  between operations  14.2 us (4%)
  other arithmetic  12.4 us (4%)
    all_to_all x1, blocking collectives, on_device(): lax.all_to_all(outgoing, 'ep', split_axis=0, concat_axis=1, tiled=True)  63.2 us
    all_to_all x2, waiting for transfers between devices, sent_and_summed(): lax.all_to_all(blocks, axis, split_axis=0, concat_axis=0, tiled=True)  62.6 us
    all_gather x1, waiting for transfers between devices, on_device(): piece = lax.all_gather(arrived, 'tp', axis=0, tiled=True)  55.8 us
    all_to_all x1, waiting for transfers between devices, on_device(): lax.all_to_all(expert_out.reshape(n_ep, capacity, width), 'ep', split_axi...  50.1 us
    dot_general x1, matrix products, on_device(): jnp.dot(piece, w_down[0], preferred_element_type=jnp.float32)  17.5 us
    all_to_all x1, starting transfers between devices, on_device(): lax.all_to_all(expert_out.reshape(n_ep, capacity, width), 'ep', split_axi...  10.7 us
    dot_general x1, matrix products, on_device(): gate_val = jnp.dot(piece, w_gate[0], preferred_element_type=jnp.float32)  9.98 us
    all_to_all x2, starting transfers between devices, sent_and_summed(): lax.all_to_all(blocks, axis, split_axis=0, concat_axis=0, tiled=True)  8.91 us
  transfers between devices with their start and end apart: 5, of which 5 were waited for; matrix products, arithmetic and copies ran while one was open for 2% of the time, Pallas kernels for 0%

commit v1 on v0

--- a/solution.py
+++ b/solution.py
@@ -1,9 +1,20 @@
+import functools
 import jax
 import jax.numpy as jnp
 from jax import lax
 from jax.sharding import PartitionSpec as P
 
 EPS = 1e-06
+
+
+def shape_the_cells(here_x, axis_id):
+    vec_out = lax.axis_size(axis_id)
+    y2 = jnp.stack([here_x] * vec_out)
+    view_out = lax.all_to_all(y2, axis_name=axis_id, split_axis=0, concat_axis=0)
+    return jnp.concatenate(view_out, axis=0)
+
+
+wrap_the_ranges = functools.partial(shape_the_cells, axis_id="tp")
 
 
 def passed_along(block, axis, distance):
@@ -85,7 +96,7 @@
     arrived = lax.all_to_all(outgoing, "ep", split_axis=0, concat_axis=1, tiled=True).reshape(
         -1, width
     )
-    piece = lax.all_gather(arrived, "tp", axis=0, tiled=True)
+    piece = wrap_the_ranges(arrived)
     gate_val = jnp.dot(piece, w_gate[0], preferred_element_type=jnp.float32)
     up_val = jnp.dot(piece, w_up[0], preferred_element_type=jnp.float32)
     hidden = (jax.nn.silu(gate_val) * up_val).astype(jnp.bfloat16)

time: 334 us -> 323 us (0.967)
  blocking collectives: 63.2 us -> 126 us
  waiting for transfers between devices: 172 us -> 111 us
  between operations: 14.2 us -> 0.88 us
    all_to_all x0 -> x1, blocking collectives: none -> 62.9 us  [shape_the_cells(): lax.all_to_all(y2, axis_name=axis_id, split_axis=0, concat_axis=0)]
    all_gather x1 -> x0, waiting for transfers between devices: 55.8 us -> none  [on_device(): piece = lax.all_gather(arrived, 'tp', axis=0, tiled=True)]
    all_to_all x2, waiting for transfers between devices: 62.6 us -> 57.7 us  [sent_and_summed(): lax.all_to_all(blocks, axis, split_axis=0, concat_axis=0, tiled=True)]
    reshape x1 -> x0, local copies, waits for them, and re-layouts: 3.66 us -> none  [on_device(): lax.all_to_all(outgoing, 'ep', split_axis=0, concat_axis=1, tiled=True)]
  transfers between devices with their start and end apart: 5 -> 4, of which waited for: 5 -> 4; matrix products, arithmetic and copies ran while one was open for 2% -> 2% of each run, Pallas kernels for 0% -> 0%
where the time goes in v1:
time: 323 us; the launch traced here: 322 us
  blocking collectives  126 us (39%)
  waiting for transfers between devices  111 us (34%)
  matrix products  26.1 us (8%)
  starting transfers between devices  23.1 us (7%)
  local copies, waits for them, and re-layouts  23 us (7%)
  other arithmetic  12.4 us (4%)
    all_to_all x1, blocking collectives, on_device(): lax.all_to_all(outgoing, 'ep', split_axis=0, concat_axis=1, tiled=True)  63.2 us
    all_to_all x1, blocking collectives, shape_the_cells(): lax.all_to_all(y2, axis_name=axis_id, split_axis=0, concat_axis=0)  62.9 us
    all_to_all x2, waiting for transfers between devices, sent_and_summed(): lax.all_to_all(blocks, axis, split_axis=0, concat_axis=0, tiled=True)  57.7 us
    all_to_all x1, waiting for transfers between devices, on_device(): lax.all_to_all(expert_out.reshape(n_ep, capacity, width), 'ep', split_axi...  50.1 us
    dot_general x1, matrix products, on_device(): jnp.dot(piece, w_down[0], preferred_element_type=jnp.float32)  17.5 us
    all_to_all x1, starting transfers between devices, on_device(): lax.all_to_all(expert_out.reshape(n_ep, capacity, width), 'ep', split_axi...  12.3 us
    all_to_all x2, starting transfers between devices, sent_and_summed(): lax.all_to_all(blocks, axis, split_axis=0, concat_axis=0, tiled=True)  8.91 us
    dot_general x1, matrix products, on_device(): gate_val = jnp.dot(piece, w_gate[0], preferred_element_type=jnp.float32)  7.14 us
  transfers between devices with their start and end apart: 4, of which 4 were waited for; matrix products, arithmetic and copies ran while one was open for 2% of the time, Pallas kernels for 0%

profile of v1, /device:TPU:8, one launch (start us, length us, event | category | flops | bytes accessed | tf_op | source)
XLA Modules:
  0.0 322.5 jit_solution(671714827138857520)
XLA Ops:
  3.7 1.4 scatter_custom_fusion
  7.7 3.0 gather_fusion
  10.7 2.4 reshape.89
  13.1 63.2 %all_to_all.32 = bf16[64,5,2048]{2,1,0:T(8,128)(2,1)} all-to-all(bf16[64,5,2048]{2,1,0:T(8,128)(2,1)S(1)} %reshape.89), channel_id=1, replica_groups=mesh['ep'=64,'tp'=4] {'ep'}, dimensions={0} | all-to-all | bytes 2621440 | tf_op jit(solution)/shard_map/all_to_all | solution.py:96
  76.3 2.6 all_to_all.23
  79.6 62.9 %all_to_all.33 = bf16[4,320,2048]{2,1,0:T(8,128)(2,1)S(1)} all-to-all(bf16[4,320,2048]{2,1,0:T(8,128)(2,1)S(1)} %stack.3), channel_id=1, replica_groups=mesh['ep'=64,'tp'=4] {'tp'}, dimensions={0} | all-to-all | bytes 10485760 | tf_op jit(solution)/shard_map/all_to_all | solution.py:13
  142.4 2.3 copy-done.1
  144.8 7.1 %fusion.2 = f32[1280,896]{1,0:T(8,128)} fusion(bf16[1280,2048]{1,0:T(8,128)(2,1)S(1)} %bitcast.49, bf16[1,2048,896]{2,1,0:T(8,128)(2,1)S(1)} %copy-done.7), kind=kOutput, calls=%fused_computation.7 | convolution fusion | flops 4697620480 | bytes 13500416 | tf_op jit(solution)/shard_map/dot_general | solution.py:100
  151.9 17.5 %convolution_convert_fusion = bf16[1280,2048]{1,0:T(8,128)(2,1)} fusion(bf16[1,896,2048]{2,1,0:T(8,128)(2,1)} %param.23, f32[1280,896]{1,0:T(8,128)} %fusion.2, bf16[1280,2048]{1,0:T(8,128)(2,1)} %bitcast.50, bf16[1,2048,896]{2,1,0:T(8,128)(2,1)} %param.22), kind=kOutput, calls=%fused_computation.3 | convolution fusion | flops 9404743680 | bytes 22413312 | tf_op jit(solution)/shard_map/dot_general | solution.py:105
  169.5 5.2 %all-to-all-start.3 = ((bf16[4,320,2048]{2,1,0:T(8,128)(2,1)}), bf16[4,320,2048]{2,1,0:T(8,128)(2,1)}, u32[]{:S(2)}, u32[]{:S(2)}) async-start(bf16[4,320,2048]{2,1,0:T(8,128)(2,1)} %bitcast.48), calls=%async_computation.3 | async-start | bytes 10485760 | tf_op jit(solution)/shard_map/all_to_all | solution.py:33
  174.8 1.9 collective-permute-start
  176.7 3.0 collective-permute-done
  179.7 1.5 convolution_convert_fusion.1
  181.1 51.3 %all-to-all-done.3 = bf16[4,320,2048]{2,1,0:T(8,128)(2,1)} async-done(((bf16[4,320,2048]{2,1,0:T(8,128)(2,1)}), bf16[4,320,2048]{2,1,0:T(8,128)(2,1)}, u32[]{:S(2)}, u32[]{:S(2)}) %all-to-all-start.3) | async-done | bytes 5242912 | tf_op jit(solution)/shard_map/all_to_all | solution.py:33
  232.4 3.7 %all-to-all-start = ((bf16[4,64,2048]{2,1,0:T(8,128)(2,1)}), bf16[4,64,2048]{2,1,0:T(8,128)(2,1)S(1)}, u32[]{:S(2)}, u32[]{:S(2)}) async-start(bf16[4,64,2048]{2,1,0:T(8,128)(2,1)} %bitcast.3), calls=%async_computation | async-start | bytes 2097152 | tf_op jit(solution)/shard_map/all_to_all | solution.py:33
  236.1 3.6 %reduce_sum.57 = bf16[320,2048]{1,0:T(8,128)(2,1)S(1)} reduce(bf16[4,320,2048]{2,1,0:T(8,128)(2,1)} %all-to-all-done.3, bf16[]{:T(256)} %constant.18.clone.1), dimensions={0}, to_apply=%region_6.7 | reduce | flops 1966080 | bytes 6553602 | tf_op jit(solution)/shard_map/reduce_sum | solution.py:34
  239.8 1.6 reshape.92
  241.4 6.4 %all-to-all-done = bf16[4,64,2048]{2,1,0:T(8,128)(2,1)S(1)} async-done(((bf16[4,64,2048]{2,1,0:T(8,128)(2,1)}), bf16[4,64,2048]{2,1,0:T(8,128)(2,1)S(1)}, u32[]{:S(2)}, u32[]{:S(2)}) %all-to-all-start) | async-done | bytes 1048608 | tf_op jit(solution)/shard_map/all_to_all | solution.py:33
  247.8 12.3 %all-to-all-start.4 = ((bf16[64,5,2048]{2,1,0:T(8,128)(2,1)}), bf16[64,5,2048]{2,1,0:T(8,128)(2,1)}, u32[]{:S(2)}, u32[]{:S(2)}) async-start(bf16[64,5,2048]{2,1,0:T(8,128)(2,1)} %reshape.92), calls=%async_computation.4 | async-start | bytes 4194304 | tf_op jit(solution)/shard_map/all_to_all | solution.py:107
  261.2 50.1 %all-to-all-done.4 = bf16[64,5,2048]{2,1,0:T(8,128)(2,1)} async-done(((bf16[64,5,2048]{2,1,0:T(8,128)(2,1)}), bf16[64,5,2048]{2,1,0:T(8,128)(2,1)}, u32[]{:S(2)}, u32[]{:S(2)}) %all-to-all-start.4) | async-done | bytes 1310752 | tf_op jit(solution)/shard_map/all_to_all | solution.py:107
  311.3 2.6 reshape.93
  313.8 2.3 gather_fusion.1
  316.2 2.4 reshape.94
  318.5 3.9 %multiply_reduce_fusion = bf16[128,2048]{1,0:T(8,128)(2,1)} fusion(f32[128,2,2048]{2,1,0:T(2,128)S(1)} %reshape.94, f32[128,2]{1,0:T(8,128)S(1)} %copy.19), kind=kLoop, calls=%fused_computation.10 | loop fusion | flops 786432 | bytes 2622464 | tf_op jit(solution)/shard_map/reduce_sum | solution.py:111
  (42 shorter events, 7.3 us)
Async XLA Ops:
  0.6 179.1 %copy-start = (bf16[256,2048]{1,0:T(8,128)(2,1)S(1)}, bf16[256,2048]{1,0:T(8,128)(2,1)}, u32[]{:S(2)}) copy-start(bf16[256,2048]{1,0:T(8,128)(2,1)} %param.16) | copy-start | bytes 3145732
  79.6 65.2 %copy-start.7 = (bf16[1,2048,896]{2,1,0:T(8,128)(2,1)S(1)}, bf16[1,2048,896]{2,1,0:T(8,128)(2,1)}, u32[]{:S(2)}) copy-start(bf16[1,2048,896]{2,1,0:T(8,128)(2,1)} %param.21) | copy-start | bytes 11010052
  142.4 2.3 copy-start.1
  169.5 5.3 %copy-start.3 = (bf16[256,256]{1,0:T(8,128)(2,1)S(1)}, bf16[256,256]{1,0:T(8,128)(2,1)}, u32[]{:S(2)}) copy-start(bf16[256,256]{1,0:T(8,128)(2,1)} %param.14) | copy-start | bytes 393220
  169.5 5.3 %copy-start.4 = (bf16[256,256]{1,0:T(8,128)(2,1)S(1)}, bf16[256,256]{1,0:T(8,128)(2,1)}, u32[]{:S(2)}) copy-start(bf16[256,256]{1,0:T(8,128)(2,1)} %param.12) | copy-start | bytes 393220
  169.5 7.2 %copy-start.5 = (f32[3,256]{1,0:T(4,128)S(1)}, f32[3,256]{1,0:T(4,128)}, u32[]{:S(2)}) copy-start(f32[3,256]{1,0:T(4,128)} %param.15) | copy-start | bytes 9220
  169.5 10.2 %copy-start.2 = (bf16[256,256]{1,0:T(8,128)(2,1)S(1)}, bf16[256,256]{1,0:T(8,128)(2,1)}, u32[]{:S(2)}) copy-start(bf16[256,256]{1,0:T(8,128)(2,1)} %param.13) | copy-start | bytes 393220
  169.5 62.9 %all-to-all-start.3 = ((bf16[4,320,2048]{2,1,0:T(8,128)(2,1)}), bf16[4,320,2048]{2,1,0:T(8,128)(2,1)}, u32[]{:S(2)}, u32[]{:S(2)}) async-start(bf16[4,320,2048]{2,1,0:T(8,128)(2,1)} %bitcast.48), calls=%async_computation.3 | async-start | bytes 10485760 | tf_op jit(solution)/shard_map/all_to_all | solution.py:33
  174.8 4.9 %collective-permute-start = (f32[2,256]{1,0:T(2,128)S(1)}, f32[2,256]{1,0:T(2,128)S(1)}, u32[]{:S(2)}, u32[]{:S(2)}) collective-permute-start(f32[2,256]{1,0:T(2,128)S(1)} %slice.36), channel_id=1, source_target_pairs={{0,4},{4,8},{8,12},{12,16},{16,20},{20,24},{24,28},{28,32},{32,36}... | collective-permute-start | bytes 6152 | tf_op jit(solution)/shard_map/ppermute | solution.py:23
  232.4 15.4 %all-to-all-start = ((bf16[4,64,2048]{2,1,0:T(8,128)(2,1)}), bf16[4,64,2048]{2,1,0:T(8,128)(2,1)S(1)}, u32[]{:S(2)}, u32[]{:S(2)}) async-start(bf16[4,64,2048]{2,1,0:T(8,128)(2,1)} %bitcast.3), calls=%async_computation | async-start | bytes 2097152 | tf_op jit(solution)/shard_map/all_to_all | solution.py:33
  239.8 20.3 %copy-start.6 = (f32[128,2]{0,1:T(2,128)S(1)}, f32[128,2]{0,1:T(2,128)}, u32[]{:S(2)}) copy-start(f32[128,2]{0,1:T(2,128)} %param.20) | copy-start | bytes 3076
  247.8 63.5 %all-to-all-start.4 = ((bf16[64,5,2048]{2,1,0:T(8,128)(2,1)}), bf16[64,5,2048]{2,1,0:T(8,128)(2,1)}, u32[]{:S(2)}, u32[]{:S(2)}) async-start(bf16[64,5,2048]{2,1,0:T(8,128)(2,1)} %reshape.92), calls=%async_computation.4 | async-start | bytes 4194304 | tf_op jit(solution)/shard_map/all_to_all | solution.py:107
